TPU v7x, 32 devices: a whole 2x2x4 slice. The times are simulated.
32 devices in a mesh: kv: 16 (over z, y, x), tp: 2 (over core).
Axes of the slice: x: 2, y: 2, z: 4, core: 2. Of those that a mesh axis runs over, the one named last changes fastest.
Arguments:
- queries: bfloat16 [4096, 1024], P('kv', 'tp'), may hold values from -4 to 4
- keys: bfloat16 [4096, 1024], P('kv', 'tp'), may hold values from -4 to 4
- values: bfloat16 [4096, 1024], P('kv', 'tp'), may hold values from -5 to 5
- log_sums: float32 [16, 4096], P('tp', 'kv'), may hold values from 5.5 to 7
- out_grad: bfloat16 [4096, 1024], P('kv', 'tp'), may hold values from -24 to 24
- chosen: int32 [32, 8], P('kv'), may hold values from -1 to 127, as said below
- normed: bfloat16 [4096, 2048], P('kv', 'tp'), may hold values from -0.23925781 to 0.23925781
Outputs:
- query_grad: bfloat16 [4096, 1024], P('kv', 'tp')
- key_grad: bfloat16 [4096, 1024], P('kv', 'tp')
- value_grad: bfloat16 [4096, 1024], P('kv', 'tp')
- weight_grad: float32 [2048, 1024], P('kv', 'tp')
Inputs may be any that keep to these rules, and one draw needn't show every extreme that they name: `chosen`: each used entry names a key block that ends at or before its query block's start; the used entries of one list are distinct. Among the lists of the 2 query blocks of one index of kv, the key blocks of any other index of kv appear as at most one distinct block; for every index from 1 on, the first query block's list names a block of the index before, and the last index's first query block's list names a block of index 0. Blocks of the own index of kv before the query block may appear freely.
All inputs are finite; a program needn't handle non-finite values.
Results may differ from a plain program's by a relative error of at most 0.008.
Values may be sent and summed in bfloat16 or wider, within the bound.
A program may use at most 64 MiB of HBM per device.

v0:
```python
from functools import partial

import jax
import jax.numpy as jnp
from jax import lax
from jax.sharding import PartitionSpec as P

QB = 128
KB = 32


def block_grads(inputs, scaling):
    query_blk, grad_blk, sums_blk, keys_sel, vals_sel, keys_own, vals_own, eligible_blocks = inputs
    span_rows = query_blk.shape[0]
    scores = (
        jnp.einsum("qhd,skhd->hqsk", query_blk, keys_sel, preferred_element_type=jnp.float32)
        * scaling
    )
    weights = jnp.where(
        eligible_blocks[None, None, :, None], jnp.exp(scores - sums_blk[:, :, None, None]), 0.0
    )
    causal = lax.broadcasted_iota(jnp.int32, (span_rows, span_rows), 0) >= lax.broadcasted_iota(
        jnp.int32, (span_rows, span_rows), 1
    )
    own_scores = (
        jnp.einsum("qhd,khd->hqk", query_blk, keys_own, preferred_element_type=jnp.float32)
        * scaling
    )
    own_weights = jnp.where(causal[None], jnp.exp(own_scores - sums_blk[:, :, None]), 0.0)
    weights_low = weights.astype(jnp.bfloat16)
    own_low = own_weights.astype(jnp.bfloat16)
    attended = jnp.einsum(
        "hqsk,skhd->qhd", weights_low, vals_sel, preferred_element_type=jnp.float32
    )
    attended = attended + jnp.einsum(
        "hqk,khd->qhd", own_low, vals_own, preferred_element_type=jnp.float32
    )
    deltas = jnp.sum(grad_blk.astype(jnp.float32) * attended, axis=-1).T
    dots_sel = jnp.einsum("qhd,skhd->hqsk", grad_blk, vals_sel, preferred_element_type=jnp.float32)
    own_dots = jnp.einsum("qhd,khd->hqk", grad_blk, vals_own, preferred_element_type=jnp.float32)
    slopes = (weights * (dots_sel - deltas[:, :, None, None])).astype(jnp.bfloat16)
    own_slopes = (own_weights * (own_dots - deltas[:, :, None])).astype(jnp.bfloat16)
    query_part = jnp.einsum("hqsk,skhd->qhd", slopes, keys_sel, preferred_element_type=jnp.float32)
    query_part = scaling * (
        query_part
        + jnp.einsum("hqk,khd->qhd", own_slopes, keys_own, preferred_element_type=jnp.float32)
    )
    key_terms = scaling * jnp.einsum(
        "hqsk,qhd->skhd", slopes, query_blk, preferred_element_type=jnp.float32
    )
    value_terms = jnp.einsum(
        "hqsk,qhd->skhd", weights_low, grad_blk, preferred_element_type=jnp.float32
    )
    own_key_terms = scaling * jnp.einsum(
        "hqk,qhd->khd", own_slopes, query_blk, preferred_element_type=jnp.float32
    )
    own_value_terms = jnp.einsum(
        "hqk,qhd->khd", own_low, grad_blk, preferred_element_type=jnp.float32
    )
    return (query_part.astype(jnp.bfloat16), key_terms, value_terms, own_key_terms, own_value_terms)


def body(queries, keys, values, log_sums, out_grad, chosen, normed):
    devices = lax.axis_size("kv")
    myself = lax.axis_index("kv")
    rows_here, columns = queries.shape
    head_count = log_sums.shape[0]
    head_size = columns // head_count
    query_blocks = rows_here // QB
    key_blocks = rows_here // KB
    selected = chosen.shape[1]
    groups = 1
    slot_count = devices * groups
    owners = chosen // key_blocks
    offsets = chosen % key_blocks
    eligible_blocks = chosen >= 0
    remote = eligible_blocks & (owners != myself)
    slot_ids = owners * groups
    matches = remote[:, :, None] & (
        slot_ids[:, :, None] == jnp.arange(slot_count, dtype=jnp.int32)[None, None, :]
    )
    wanted = jnp.max(jnp.where(matches, offsets[:, :, None] + 1, 0), axis=(0, 1))
    requested = lax.all_to_all(
        wanted.reshape(devices, groups), "kv", split_axis=0, concat_axis=0, tiled=True
    ).reshape(-1)
    live_request = requested > 0
    picked = jnp.clip(requested - 1, 0, key_blocks - 1)
    key_table = keys.reshape(key_blocks, KB, columns)
    value_table = values.reshape(key_blocks, KB, columns)
    zero_block = jnp.zeros((), keys.dtype)
    outgoing_keys = jnp.where(live_request[:, None, None], key_table[picked], zero_block).reshape(
        devices, groups, KB, columns
    )
    outgoing_values = jnp.where(
        live_request[:, None, None], value_table[picked], zero_block
    ).reshape(devices, groups, KB, columns)
    fetched_keys, fetched_values = (
        lax.all_to_all(outgoing_keys, "kv", split_axis=0, concat_axis=0, tiled=True),
        lax.all_to_all(outgoing_values, "kv", split_axis=0, concat_axis=0, tiled=True),
    )
    all_keys = jnp.concatenate([fetched_keys.reshape(slot_count, KB, columns), key_table], axis=0)
    all_values = jnp.concatenate(
        [fetched_values.reshape(slot_count, KB, columns), value_table], axis=0
    )
    table_ids = jnp.where(remote, slot_ids, jnp.where(eligible_blocks, slot_count + offsets, 0))
    keys_sel = all_keys[table_ids].reshape(query_blocks, selected, KB, head_count, head_size)
    vals_sel = all_values[table_ids].reshape(query_blocks, selected, KB, head_count, head_size)
    block_shape = (query_blocks, QB, head_count, head_size)
    inputs = (
        queries.reshape(block_shape),
        out_grad.reshape(block_shape),
        log_sums.reshape(head_count, query_blocks, QB).transpose(1, 0, 2),
        keys_sel,
        vals_sel,
        keys.reshape(block_shape),
        values.reshape(block_shape),
        eligible_blocks,
    )
    query_part, key_terms, value_terms, own_key_terms, own_value_terms = lax.map(
        partial(block_grads, scaling=head_size ** (-0.5)), inputs
    )
    routes = (
        table_ids.reshape(-1)[:, None]
        == jnp.arange(slot_count + key_blocks, dtype=jnp.int32)[None, :]
    ) & eligible_blocks.reshape(-1)[:, None]
    stacked_terms = jnp.stack(
        [key_terms.reshape(-1, KB * columns), value_terms.reshape(-1, KB * columns)]
    )
    routed = jnp.einsum(
        "ab,xac->xbc", routes.astype(jnp.float32), stacked_terms, precision=lax.Precision.HIGHEST
    )
    back_keys = routed[0, :slot_count].reshape(devices, groups, KB, columns)
    back_values = routed[1, :slot_count].reshape(devices, groups, KB, columns)
    returned_keys, returned_values = (
        lax.all_to_all(back_keys, "kv", split_axis=0, concat_axis=0, tiled=True),
        lax.all_to_all(back_values, "kv", split_axis=0, concat_axis=0, tiled=True),
    )
    matched = (
        ((requested - 1)[:, None] == jnp.arange(key_blocks, dtype=jnp.int32)[None, :])
        & live_request[:, None]
    ).astype(jnp.float32)
    stacked_back = jnp.stack(
        [
            returned_keys.reshape(slot_count, KB * columns),
            returned_values.reshape(slot_count, KB * columns),
        ]
    )
    arrived = jnp.einsum("ab,xac->xbc", matched, stacked_back, precision=lax.Precision.HIGHEST)
    totals = arrived + routed[:, slot_count:]
    key_grad = (
        totals[0].reshape(rows_here, columns) + own_key_terms.reshape(rows_here, columns)
    ).astype(jnp.bfloat16)
    value_grad = (
        totals[1].reshape(rows_here, columns) + own_value_terms.reshape(rows_here, columns)
    ).astype(jnp.bfloat16)
    features_all = lax.all_gather(normed, "tp", axis=1, tiled=True)
    weight_grad = lax.psum_scatter(
        lax.dot_general(
            features_all, value_grad, (((0,), (0,)), ((), ())), preferred_element_type=jnp.float32
        ),
        "kv",
        scatter_dimension=0,
        tiled=True,
    )
    return (query_part.reshape(rows_here, columns), key_grad, value_grad, weight_grad)


def solution(mesh):
    in_specs = (
        P("kv", "tp"),
        P("kv", "tp"),
        P("kv", "tp"),
        P("tp", "kv"),
        P("kv", "tp"),
        P("kv", None),
        P("kv", "tp"),
    )
    out_specs = (P("kv", "tp"), P("kv", "tp"), P("kv", "tp"), P("kv", "tp"))
    return jax.shard_map(body, mesh=mesh, in_specs=in_specs, out_specs=out_specs, check_vma=False)
```

profile of v0, /device:TPU:0, one launch (start us, length us, event | category | flops | bytes accessed | tf_op | source)
XLA Modules:
  0.0 302.4 jit_solution(817550221960606764)
XLA Ops:
  8.1 15.4 %all_to_all.29 = s32[16,1,1]{2,1,0:T(1,128)S(1)} all-to-all(s32[16,1,1]{2,1,0:T(1,128)S(1)} %copy.86), channel_id=1, replica_groups=mesh['kv'=16,'tp'=2] {'kv'}, dimensions={0} | all-to-all | bytes 128 | tf_op jit(solution)/shard_map/all_to_all | solution.py:83
  24.2 1.5 gather_fusion.2
  25.7 1.5 gather_fusion
  28.6 16.8 %all_to_all.30 = bf16[16,1,32,512]{3,2,1,0:T(8,128)(2,1)S(1)} all-to-all(bf16[16,1,32,512]{3,2,1,0:T(8,128)(2,1)S(1)} %get-tuple-element.203), channel_id=1, replica_groups=mesh['kv'=16,'tp'=2] {'kv'}, dimensions={0} | all-to-all | bytes 1048576 | tf_op jit(solution)/shard_map/all_to_all | solution.py:98
  45.3 3.9 %all-to-all-start.2 = ((bf16[16,1,32,512]{3,2,1,0:T(8,128)(2,1)}), bf16[16,1,32,512]{3,2,1,0:T(8,128)(2,1)S(1)}, u32[]{:S(2)}, u32[]{:S(2)}) async-start(bf16[16,1,32,512]{3,2,1,0:T(8,128)(2,1)} %get-tuple-element.202), calls=%async_computation.2 | async-start | bytes 1048576 | tf_op jit(solution)/shard_map/all_to_all | solution.py:99
  52.0 1.3 copy.92
  55.7 2.0 copy.95
  60.0 3.3 %all-to-all-done.2 = bf16[16,1,32,512]{3,2,1,0:T(8,128)(2,1)S(1)} async-done(((bf16[16,1,32,512]{3,2,1,0:T(8,128)(2,1)}), bf16[16,1,32,512]{3,2,1,0:T(8,128)(2,1)S(1)}, u32[]{:S(2)}, u32[]{:S(2)}) %all-to-all-start.2) | async-done | bytes 524320 | tf_op jit(solution)/shard_map/all_to_all | solution.py:99
  64.5 56.6 %while.18 = (s32[]{:T(128)}, bf16[2,128,8,64]{1,3,2,0:T(8,128)(2,1)}, f32[2,8,32,8,64]{4,3,2,1,0:T(8,128)}, f32[2,8,32,8,64]{4,3,2,1,0:T(8,128)}, f32[2,128,8,64...) while((s32[]{:T(128)}, ...), condition=%wide.region_3.4_spmd, body=%wide.region_1.3_spmd.sunk | while | flops 306330624 | bytes 43585888 | solution.py:119
  70.4 1.9 fusion.160
  74.5 1.9 copy_dynamic-update-slice_fusion.3
  78.4 7.1 %dynamic_update_slice.27 = f32[2,128,8,64]{1,0,3,2:T(2,128)} dynamic-update-slice(f32[2,128,8,64]{1,0,3,2:T(2,128)} %get-tuple-element.313, f32[1,128,8,64]{1,0,3,2:T(1,128)S(1)} %bitcast.262, s32[]{:T(128)S(6)} %copy.169, s32[]{:T(128)} %constant.73.clone.1..sunk, s32[]{:T(128)} %constant.73.clone.1..sunk, s32[]{:T(128)} %constant.73.clone.1..sunk) | dynamic-update-slice | bytes 524292 | tf_op jit(solution)/shard_map/while/body/jit(dynamic_update_index_in_dim)/dynamic_update_slice | solution.py:119
  85.7 7.1 %dynamic_update_slice.28 = f32[2,128,8,64]{1,0,3,2:T(2,128)} dynamic-update-slice(f32[2,128,8,64]{1,0,3,2:T(2,128)} %get-tuple-element.314, f32[1,128,8,64]{1,0,3,2:T(1,128)S(1)} %bitcast.261, s32[]{:T(128)S(6)} %copy.169, s32[]{:T(128)} %constant.73.clone.1..sunk, s32[]{:T(128)} %constant.73.clone.1..sunk, s32[]{:T(128)} %constant.73.clone.1..sunk) | dynamic-update-slice | bytes 524292 | tf_op jit(solution)/shard_map/while/body/jit(dynamic_update_index_in_dim)/dynamic_update_slice | solution.py:119
  98.7 1.9 fusion.160
  102.8 1.9 copy_dynamic-update-slice_fusion.3
  106.7 7.1 %dynamic_update_slice.27 = f32[2,128,8,64]{1,0,3,2:T(2,128)} dynamic-update-slice(f32[2,128,8,64]{1,0,3,2:T(2,128)} %get-tuple-element.313, f32[1,128,8,64]{1,0,3,2:T(1,128)S(1)} %bitcast.262, s32[]{:T(128)S(6)} %copy.169, s32[]{:T(128)} %constant.73.clone.1..sunk, s32[]{:T(128)} %constant.73.clone.1..sunk, s32[]{:T(128)} %constant.73.clone.1..sunk) | dynamic-update-slice | bytes 524292 | tf_op jit(solution)/shard_map/while/body/jit(dynamic_update_index_in_dim)/dynamic_update_slice | solution.py:119
  114.0 7.1 %dynamic_update_slice.28 = f32[2,128,8,64]{1,0,3,2:T(2,128)} dynamic-update-slice(f32[2,128,8,64]{1,0,3,2:T(2,128)} %get-tuple-element.314, f32[1,128,8,64]{1,0,3,2:T(1,128)S(1)} %bitcast.261, s32[]{:T(128)S(6)} %copy.169, s32[]{:T(128)} %constant.73.clone.1..sunk, s32[]{:T(128)} %constant.73.clone.1..sunk, s32[]{:T(128)} %constant.73.clone.1..sunk) | dynamic-update-slice | bytes 524292 | tf_op jit(solution)/shard_map/while/body/jit(dynamic_update_index_in_dim)/dynamic_update_slice | solution.py:119
  121.2 3.3 %stack_reshape.13 = f32[1,16,16384]{2,1,0:T(8,128)} reshape(f32[2,8,32,8,64]{4,3,2,1,0:T(8,128)} %get-tuple-element.82) | data formatting | bytes 2097152 | tf_op jit(solution)/shard_map/stack;reshape | solution.py:126
  124.5 1.6 stack_reshape.12
  126.1 3.1 %convolution_bitcast_fusion.2 = f32[2,24,16384]{2,1,0:T(8,128)S(1)} fusion(f32[1,16,16384]{2,1,0:T(8,128)} %stack_reshape.13, f32[1,16,16384]{2,1,0:T(8,128)} %stack_reshape.12, s32[16]{0:T(128)S(1)} %eq.46, pred[16]{0:T(512)(128)(4,1)S(1)} %and.45), kind=kOutput, calls=%fused_computation.80 | convolution fusion | flops 151520000 | bytes 5242960 | tf_op jit(solution)/shard_map/ab,xac->xbc/dot_general | solution.py:129
  130.3 1.6 copy.133
  131.9 4.3 %all-to-all-start.4 = ((f32[16,1,32,512]{3,2,1,0:T(8,128)}), f32[16,1,32,512]{3,2,1,0:T(8,128)}, u32[]{:S(2)}, u32[]{:S(2)}) async-start(f32[16,1,32,512]{3,2,1,0:T(8,128)} %bitcast.264), calls=%async_computation.4 | async-start | bytes 2097152 | tf_op jit(solution)/shard_map/all_to_all | solution.py:136
  136.3 2.8 copy.132
  139.1 20.0 %all-to-all-done.4 = f32[16,1,32,512]{3,2,1,0:T(8,128)} async-done(((f32[16,1,32,512]{3,2,1,0:T(8,128)}), f32[16,1,32,512]{3,2,1,0:T(8,128)}, u32[]{:S(2)}, u32[]{:S(2)}) %all-to-all-start.4) | async-done | bytes 1048608 | tf_op jit(solution)/shard_map/all_to_all | solution.py:136
  159.1 6.1 %all-to-all-start.3 = ((f32[16,1,32,512]{3,2,1,0:T(8,128)}), f32[16,1,32,512]{3,2,1,0:T(8,128)}, u32[]{:S(2)}, u32[]{:S(2)}) async-start(f32[16,1,32,512]{3,2,1,0:T(8,128)} %bitcast.263), calls=%async_computation.3 | async-start | bytes 2097152 | tf_op jit(solution)/shard_map/all_to_all | solution.py:135
  166.0 2.4 stack_reshape.15
  168.4 19.8 %all-to-all-done.3 = f32[16,1,32,512]{3,2,1,0:T(8,128)} async-done(((f32[16,1,32,512]{3,2,1,0:T(8,128)}), f32[16,1,32,512]{3,2,1,0:T(8,128)}, u32[]{:S(2)}, u32[]{:S(2)}) %all-to-all-start.3) | async-done | bytes 1048608 | tf_op jit(solution)/shard_map/all_to_all | solution.py:135
  188.1 2.4 stack_reshape.14
  190.5 2.3 fusion.59
  194.0 3.9 %convolution_bitcast_fusion.4 = f32[2048,512]{0,1:T(8,128)} fusion(bf16[256,512]{0,1:T(8,128)(2,1)S(1)} %fusion.66, bf16[256,2048]{1,0:T(8,128)(2,1)} %all-gather.2.cloned.1.call-done), kind=kOutput, calls=%fused_computation.83 | convolution fusion | flops 536870912 | bytes 5505024 | tf_op jit(solution)/shard_map/dot_general | solution.py:158
  202.4 91.4 %reduce-scatter.2.cloned.1.call-done = f32[128,512]{0,1:T(8,128)} async-done(((f32[2048,512]{0,1:T(8,128)}), f32[128,512]{0,1:T(8,128)}) %reduce-scatter.2.cloned.1.call-update) | async-done | bytes 262160 | tf_op jit(solution)/shard_map/reduce_scatter | solution.py:157
  293.8 1.8 copy.109
  (121 shorter events, 39.0 us)
Async XLA Ops:
  27.6 21.7 %copy-start.1 = (bf16[256,512]{1,0:T(8,128)(2,1)S(1)}, bf16[256,512]{1,0:T(8,128)(2,1)}, u32[]{:S(2)}) copy-start(bf16[256,512]{1,0:T(8,128)(2,1)} %param.11) | copy-start | bytes 786436
  27.6 22.8 %copy-start = (bf16[256,512]{1,0:T(8,128)(2,1)S(1)}, bf16[256,512]{1,0:T(8,128)(2,1)}, u32[]{:S(2)}) copy-start(bf16[256,512]{1,0:T(8,128)(2,1)} %param.10) | copy-start | bytes 786436
  28.6 22.3 %copy-start.9 = (bf16[256,512]{1,0:T(8,128)(2,1)S(1)}, bf16[256,512]{1,0:T(8,128)(2,1)}, u32[]{:S(2)}) copy-start(bf16[256,512]{1,0:T(8,128)(2,1)} %param.9) | copy-start | bytes 786436
  45.3 7.9 %copy-start.10 = (bf16[256,512]{1,0:T(8,128)(2,1)S(1)}, bf16[256,512]{1,0:T(8,128)(2,1)}, u32[]{:S(2)}) copy-start(bf16[256,512]{1,0:T(8,128)(2,1)} %param.13) | copy-start | bytes 786436
  45.3 18.0 %all-to-all-start.2 = ((bf16[16,1,32,512]{3,2,1,0:T(8,128)(2,1)}), bf16[16,1,32,512]{3,2,1,0:T(8,128)(2,1)S(1)}, u32[]{:S(2)}, u32[]{:S(2)}) async-start(bf16[16,1,32,512]{3,2,1,0:T(8,128)(2,1)} %get-tuple-element.202), calls=%async_computation.2 | async-start | bytes 1048576 | tf_op jit(solution)/shard_map/all_to_all | solution.py:99
  63.3 1.2 copy-start.11
  72.2 1.6 copy-start.5
  72.5 2.0 copy-start.2
  76.4 1.3 copy-start.3
  76.4 1.9 copy-start.6
  100.5 1.6 copy-start.5
  100.8 2.0 copy-start.2
  104.7 1.3 copy-start.3
  104.7 1.9 copy-start.6
  121.2 3.3 %copy-start.4 = (f32[2,8,32,8,64]{4,3,2,1,0:T(8,128)S(1)}, f32[2,8,32,8,64]{4,3,2,1,0:T(8,128)}, u32[]{:S(2)}) copy-start(f32[2,8,32,8,64]{4,3,2,1,0:T(8,128)} %get-tuple-element.81) | copy-start | bytes 3145732
  131.9 27.1 %all-to-all-start.4 = ((f32[16,1,32,512]{3,2,1,0:T(8,128)}), f32[16,1,32,512]{3,2,1,0:T(8,128)}, u32[]{:S(2)}, u32[]{:S(2)}) async-start(f32[16,1,32,512]{3,2,1,0:T(8,128)} %bitcast.264), calls=%async_computation.4 | async-start | bytes 2097152 | tf_op jit(solution)/shard_map/all_to_all | solution.py:136
  159.1 29.1 %all-to-all-start.3 = ((f32[16,1,32,512]{3,2,1,0:T(8,128)}), f32[16,1,32,512]{3,2,1,0:T(8,128)}, u32[]{:S(2)}, u32[]{:S(2)}) async-start(f32[16,1,32,512]{3,2,1,0:T(8,128)} %bitcast.263), calls=%async_computation.3 | async-start | bytes 2097152 | tf_op jit(solution)/shard_map/all_to_all | solution.py:135
  165.2 28.9 %all-gather.2.cloned.1.call-start = ((), (), s32[]{:S(2)}) async-start(), calls=%async_computation.6 | async-start | bytes 1572864 | tf_op jit(solution)/shard_map/all_gather | solution.py:156
  165.9 127.9 %reduce-scatter.2.cloned.1.call-start = ((), (), s32[]{:S(2)}) async-start(), calls=%async_computation.7 | async-start | bytes 4456448 | tf_op jit(solution)/shard_map/reduce_scatter | solution.py:157
  192.9 1.0 copy-start.8
  197.9 3.5 %copy-start.7 = (f32[2,128,8,64]{1,0,3,2:T(2,128)S(1)}, f32[2,128,8,64]{1,0,3,2:T(2,128)}, u32[]{:S(2)}) copy-start(f32[2,128,8,64]{1,0,3,2:T(2,128)} %get-tuple-element.83) | copy-start | bytes 1572868
Sparse Core Ops, SparseCore 0:
  167.5 10.2 all-gather.1
  198.1 95.6 reduce-scatter.1
where the time goes:
time: 305 us; the launch traced here: 302 us
  waiting for transfers between devices  135 us (44%)
  local copies, waits for them, and re-layouts  76.8 us (25%)
  blocking collectives  32.2 us (11%)
  matrix products  24.7 us (8%)
  starting transfers between devices  14.5 us (5%)
  between operations  14.3 us (5%)
  other arithmetic  4.52 us (1%)
    reduce_scatter x1, waiting for transfers between devices, body(): lax.psum_scatter(lax.dot_general(features_all, value_grad, (((0,), (0,)),...  91.4 us
    dynamic_update_slice x6, local copies, waits for them, and re-layouts, body(): lax.map(partial(block_grads, scaling=head_size ** (-0.5)), inputs)  32.3 us
    all_to_all x1, waiting for transfers between devices, body(): lax.all_to_all(back_values, 'kv', split_axis=0, concat_axis=0, tiled=True)  20 us
    all_to_all x1, waiting for transfers between devices, body(): lax.all_to_all(back_keys, 'kv', split_axis=0, concat_axis=0, tiled=True)  19.8 us
    all_to_all x1, blocking collectives, body(): lax.all_to_all(outgoing_keys, 'kv', split_axis=0, concat_axis=0, tiled=True)  16.8 us
    all_to_all x1, blocking collectives, body(): lax.all_to_all(wanted.reshape(devices, groups), 'kv', split_axis=0, conca...  15.4 us
    unnamed x23, local copies, waits for them, and re-layouts  10.9 us
    while x16, local copies, waits for them, and re-layouts  6.63 us
  transfers between devices with their start and end apart: 5, of which 4 were waited for; matrix products, arithmetic and copies ran while one was open for 8% of the time, Pallas kernels for 0%

commit v1 on v0

v1 whole, which is shorter than its diff:
```python
from functools import partial

import jax
import jax.numpy as jnp
from jax import lax
from jax.experimental import pallas as pl
from jax.experimental.pallas import tpu as pltpu
from jax.sharding import PartitionSpec as P

QB = 128
KB = 32
LANES = 128
CHUNK = 256
NEG = -1e30
F32 = jnp.float32
BF16 = jnp.bfloat16


def dot(a, b, ca, cb):
    return lax.dot_general(a, b, (((ca,), (cb,)), ((), ())), preferred_element_type=F32)


def kernel(
    n, nt, hs,
    q_ref, k_ref, v_ref, lse_ref, g_ref, req_ref, used_ref, x_ref,
    qg_ref, kg_ref, vg_ref, wg_ref,
    reqbox, sel, outk, outv, kall, vall, rvo, rko, rvi, rki, wscr, ownv, ownk, bias, xall, wpart, win,
    req_s, req_r, k_s, k_r, v_s, v_r, vt_s, vt_r, kt_s, kt_r, w_s, w_r, x_s, x_r,
):
    me = lax.axis_index("kv")
    mt = lax.axis_index("tp")
    rows, cols = q_ref.shape
    nf = n * KB
    feats = x_ref.shape[1]
    wrows = wg_ref.shape[0]
    scale = hs ** (-0.5)
    hp = LANES // hs

    def rcopy(src, dst, ss, rs, dev):
        return pltpu.make_async_remote_copy(
            src_ref=src, dst_ref=dst, send_sem=ss, recv_sem=rs,
            device_id=dev, device_id_type=pl.DeviceIdType.MESH,
        )

    def slot(ref, i):
        return ref.at[pl.ds(pl.multiple_of(i * KB, KB), KB)]

    reqbox[...] = jnp.zeros_like(reqbox)
    kall[0:nf] = jnp.zeros((nf, cols), BF16)
    vall[0:nf] = jnp.zeros((nf, cols), BF16)
    rvi[...] = jnp.zeros_like(rvi)
    rki[...] = jnp.zeros_like(rki)

    barrier = pltpu.get_barrier_semaphore()

    @pl.loop(1, n)
    def _(d):
        pl.semaphore_signal(barrier, inc=1, device_id={"kv": lax.rem(me + d, n)},
                            device_id_type=pl.DeviceIdType.MESH)

    @pl.loop(1, nt)
    def _(d):
        pl.semaphore_signal(barrier, inc=1, device_id={"tp": lax.rem(mt + d, nt)},
                            device_id_type=pl.DeviceIdType.MESH)

    pl.semaphore_wait(barrier, n - 1 + nt - 1)

    def req_copy(src_i, dst_i):
        return rcopy(req_ref, reqbox.at[src_i], req_s.at[dst_i], req_r.at[src_i], {"kv": dst_i})

    def k_copy(src_i, dst_i):
        return rcopy(slot(outk, dst_i), slot(kall, src_i), k_s.at[dst_i], k_r.at[src_i], {"kv": dst_i})

    def v_copy(src_i, dst_i):
        return rcopy(slot(outv, dst_i), slot(vall, src_i), v_s.at[dst_i], v_r.at[src_i], {"kv": dst_i})

    def vt_copy(src_i, dst_i):
        return rcopy(slot(rvo, dst_i), slot(rvi, src_i), vt_s.at[dst_i], vt_r.at[src_i], {"kv": dst_i})

    def kt_copy(src_i, dst_i):
        return rcopy(slot(rko, dst_i), slot(rki, src_i), kt_s.at[dst_i], kt_r.at[src_i], {"kv": dst_i})

    def w_copy(src_i, dst_i):
        return rcopy(wpart.at[pl.ds(pl.multiple_of(dst_i * wrows, wrows), wrows)], win.at[src_i],
                     w_s.at[dst_i], w_r.at[src_i], {"kv": dst_i})

    def x_copy(src_t, dst_t):
        return rcopy(x_ref, xall.at[src_t], x_s.at[dst_t], x_r.at[src_t], {"tp": dst_t})

    @pl.loop(0, me)
    def _(j):
        req_copy(me, j).start()

    @pl.loop(1, nt)
    def _(d):
        x_copy(mt, lax.rem(mt + d, nt)).start()

    kall[nf:] = k_ref[...]
    vall[nf:] = v_ref[...]
    xall[mt] = x_ref[...]
    used = used_ref[...]
    nslots = used.shape[0]
    bias[...] = jnp.broadcast_to(used, (nslots, KB, rows)).reshape(nslots * KB, rows)
    kpos = lax.broadcasted_iota(jnp.int32, (rows, rows), 0)
    qpos = lax.broadcasted_iota(jnp.int32, (rows, rows), 1)
    causal = (kpos <= qpos) & (kpos // QB == qpos // QB)
    bias[nf:] = jnp.where(causal, 0.0, bias[nf:])

    @pl.loop(me + 1, n)
    def _(i):
        req_copy(i, me).wait_recv()

    box = reqbox[:, 0:1, :]
    lane = lax.broadcasted_iota(jnp.int32, box.shape, 2)
    off = jnp.sum(jnp.where(lane == me, box, 0), axis=2, keepdims=True)
    row3 = lax.broadcasted_iota(jnp.int32, (n, KB, rows), 1)
    col3 = lax.broadcasted_iota(jnp.int32, (n, KB, rows), 2)
    hit = jnp.where(col3 == (off - 1) * KB + row3, 1.0, 0.0)
    sel[...] = hit.reshape(nf, rows).astype(BF16)

    outk[...] = dot(sel[...], k_ref[...], 1, 0).astype(BF16)

    @pl.loop(me + 1, n)
    def _(i):
        k_copy(me, i).start()

    outv[...] = dot(sel[...], v_ref[...], 1, 0).astype(BF16)

    @pl.loop(me + 1, n)
    def _(i):
        v_copy(me, i).start()

    lane_ids = lax.broadcasted_iota(jnp.int32, (1, LANES), 1)
    masks = [
        jnp.where((lane_ids >= s * hs) & (lane_ids < (s + 1) * hs), 1.0, 0.0).astype(BF16)
        for s in range(hp)
    ]

    @pl.loop(0, me)
    def _(j):
        k_copy(j, me).wait_recv()

    for p in range(cols // LANES):
        at = slice(p * LANES, (p + 1) * LANES)
        qp = q_ref[:, at] * jnp.asarray(scale, BF16)
        gp = g_ref[:, at]
        kp = kall[:, at]
        terms = None
        for s in range(hp):
            h = p * hp + s
            scores = dot(kp, qp * masks[s], 1, 1)
            w = jnp.exp(scores + (bias[...] - lse_ref[h:h + 1, :]))
            wscr[h] = w
            term = dot(w.astype(BF16), gp * masks[s], 1, 0)
            terms = term if terms is None else terms + term
        rvo[:, at] = terms[:nf].astype(BF16)
        ownv[:, at] = terms[nf:]

    @pl.loop(0, me)
    def _(j):
        vt_copy(me, j).start()

    @pl.loop(0, me)
    def _(j):
        v_copy(j, me).wait_recv()

    sub = lax.broadcasted_iota(jnp.int32, (LANES, rows), 0)
    for p in range(cols // LANES):
        at = slice(p * LANES, (p + 1) * LANES)
        qp = q_ref[:, at] * jnp.asarray(scale, BF16)
        gp = g_ref[:, at]
        kp = kall[:, at]
        vp = vall[:, at]
        terms = None
        grads = None
        for s in range(hp):
            h = p * hp + s
            dots = dot(vp, gp * masks[s], 1, 1)
            w = wscr[h]
            deltas = jnp.sum(w.astype(BF16).astype(F32) * dots, axis=0, keepdims=True)
            slopes = (w * (dots - deltas)).astype(BF16)
            term = dot(slopes, qp * masks[s], 1, 0)
            terms = term if terms is None else terms + term
            part = dot(kp, slopes, 0, 0)
            grads = part if grads is None else jnp.where(sub >= s * hs, part, grads)
        rko[:, at] = terms[:nf].astype(BF16)
        ownk[:, at] = terms[nf:]
        qg_ref[:, at] = (grads * scale).T.astype(BF16)

    @pl.loop(0, me)
    def _(j):
        kt_copy(me, j).start()

    @pl.loop(me + 1, n)
    def _(i):
        vt_copy(i, me).wait_recv()

    vg = (ownv[...] + dot(sel[...], rvi[...], 0, 0)).astype(BF16)
    vg_ref[...] = vg

    @pl.loop(1, nt)
    def _(d):
        x_copy(lax.rem(mt + d, nt), mt).wait_recv()

    width = min(CHUNK, feats)
    for t in range(nt):
        for c in range(feats // width):
            piece = dot(xall[t, :, c * width:(c + 1) * width], vg, 0, 0)
            wpart[t * feats + c * width:t * feats + (c + 1) * width, :] = piece.astype(BF16)

    @pl.loop(1, n)
    def _(d):
        w_copy(me, lax.rem(me + d, n)).start()

    @pl.loop(me + 1, n)
    def _(i):
        kt_copy(i, me).wait_recv()

    kg_ref[...] = (ownk[...] + dot(sel[...], rki[...], 0, 0)).astype(BF16)

    wg_ref[...] = wpart[pl.ds(pl.multiple_of(me * wrows, wrows), wrows), :].astype(F32)

    @pl.loop(1, n)
    def _(d):
        i = lax.rem(me + n - d, n)
        w_copy(i, me).wait_recv()
        wg_ref[...] += win[i].astype(F32)

    @pl.loop(0, me)
    def _(j):
        req_copy(me, j).wait_send()
        vt_copy(me, j).wait_send()
        kt_copy(me, j).wait_send()

    @pl.loop(me + 1, n)
    def _(i):
        k_copy(me, i).wait_send()
        v_copy(me, i).wait_send()

    @pl.loop(1, n)
    def _(d):
        w_copy(me, lax.rem(me + d, n)).wait_send()

    @pl.loop(1, nt)
    def _(d):
        x_copy(mt, lax.rem(mt + d, nt)).wait_send()


def body(n, nt, queries, keys, values, log_sums, out_grad, chosen, normed):
    me = lax.axis_index("kv")
    rows, cols = queries.shape
    heads = log_sums.shape[0]
    hs = cols // heads
    key_blocks = rows // KB
    nf = n * KB
    feats = normed.shape[1]
    wrows = feats * nt // n
    owners = chosen // key_blocks
    offsets = chosen % key_blocks
    valid = chosen >= 0
    remote = valid & (owners != me)
    ids = jnp.where(remote, owners, jnp.where(valid, n + offsets, -1))
    lanes = jnp.arange(LANES, dtype=jnp.int32)
    wanted = jnp.max(
        jnp.where(remote[:, :, None] & (owners[:, :, None] == lanes), offsets[:, :, None] + 1, 0),
        axis=(0, 1),
    )
    req = jnp.broadcast_to(wanted[None, :], (8, LANES))
    slots = jnp.arange(n + key_blocks, dtype=jnp.int32)
    use = jnp.any(ids[:, :, None] == slots, axis=1).T
    used = jnp.repeat(jnp.where(use, 0.0, NEG).astype(F32), QB, axis=1)[:, None, :]
    vmem = pl.BlockSpec(memory_space=pltpu.VMEM)
    dma = pltpu.SemaphoreType.DMA
    return pl.pallas_call(
        partial(kernel, n, nt, hs),
        out_shape=(
            jax.ShapeDtypeStruct((rows, cols), BF16),
            jax.ShapeDtypeStruct((rows, cols), BF16),
            jax.ShapeDtypeStruct((rows, cols), BF16),
            jax.ShapeDtypeStruct((wrows, cols), F32),
        ),
        in_specs=[vmem] * 8,
        out_specs=(vmem,) * 4,
        scratch_shapes=[
            pltpu.VMEM((n, 8, LANES), jnp.int32),
            pltpu.VMEM((nf, rows), BF16),
            pltpu.VMEM((nf, cols), BF16),
            pltpu.VMEM((nf, cols), BF16),
            pltpu.VMEM((nf + rows, cols), BF16),
            pltpu.VMEM((nf + rows, cols), BF16),
            pltpu.VMEM((nf, cols), BF16),
            pltpu.VMEM((nf, cols), BF16),
            pltpu.VMEM((nf, cols), BF16),
            pltpu.VMEM((nf, cols), BF16),
            pltpu.VMEM((heads, nf + rows, rows), F32),
            pltpu.VMEM((rows, cols), F32),
            pltpu.VMEM((rows, cols), F32),
            pltpu.VMEM((nf + rows, rows), F32),
            pltpu.VMEM((nt, rows, feats), BF16),
            pltpu.VMEM((n * wrows, cols), BF16),
            pltpu.VMEM((n, wrows, cols), BF16),
        ] + [dma((n,))] * 12 + [dma((nt,))] * 2,
        compiler_params=pltpu.CompilerParams(
            collective_id=0, has_side_effects=True, vmem_limit_bytes=60 * 1024 * 1024
        ),
    )(queries, keys, values, log_sums, out_grad, req, used, normed)


def solution(mesh):
    in_specs = (
        P("kv", "tp"),
        P("kv", "tp"),
        P("kv", "tp"),
        P("tp", "kv"),
        P("kv", "tp"),
        P("kv", None),
        P("kv", "tp"),
    )
    out_specs = (P("kv", "tp"), P("kv", "tp"), P("kv", "tp"), P("kv", "tp"))
    fn = partial(body, mesh.shape["kv"], mesh.shape["tp"])
    return jax.shard_map(fn, mesh=mesh, in_specs=in_specs, out_specs=out_specs, check_vma=False)
```

time: 305 us -> 103 us (0.34)
  the two profiles are of different devices: /device:TPU:0 before, /device:TPU:14 now
where the time goes in v1:
time: 103 us
  Pallas kernels  95.8 us (93%)
  local copies, waits for them, and re-layouts  6.56 us (6%)
    pallas_call x1, Pallas kernels, body(): pl.pallas_call(partial(kernel, n, nt, hs), out_shape=(jax.ShapeDtypeStruc...  95.8 us
    unnamed x12, local copies, waits for them, and re-layouts  5.18 us

profile of v1, /device:TPU:14, one launch (start us, length us, event | category | flops | bytes accessed | tf_op | source)
XLA Modules:
  0.0 103.2 jit_solution(7813097992590796929)
XLA Ops:
  0.6 0.0 copy-start.3
  0.6 0.7 copy-done.3
  1.3 0.1 fusion.1
  1.4 0.1 select_reduce_fusion
  1.5 0.6 broadcast_in_dim.39.req_ref
  2.1 0.1 copy.11
  2.2 0.7 broadcast_in_dim.42
  2.9 95.8 %shard_map.102 = (bf16[256,512]{1,0:T(8,128)(2,1)}, bf16[256,512]{1,0:T(8,128)(2,1)}, bf16[256,512]{1,0:T(8,128)(2,1)}, f32[128,512]{1,0:T(8,128)}) custom-call(bf16[256,512]{1,0:T(8,128)(2,1)} %q_ref.1, bf16[256,512]{1,0:T(8,128)(2,1)} %k_ref.1, bf16[256,512]{1,0:T(8,128)(2,1)} %v_ref.1, f32[8,256]{1,0:T(8,128)} %lse_ref.1, bf16[256,512]{1,0:T(8,128)(2,1)} %g_ref.1, ...), custom_call_target="tpu_custom_call" | custom-call | tf_op jit(solution)/shard_map/pallas_call | solution.py:274
  98.7 0.0 copy-start.2
  98.7 1.7 %copy.16 = bf16[256,512]{1,0:T(8,128)(2,1)} copy(bf16[256,512]{1,0:T(8,128)(2,1)} %get-tuple-element.11) | data formatting | bytes 524288
  100.4 0.0 copy-done.2
  100.4 0.0 copy-start.1
  100.4 0.7 copy.17
  101.1 0.3 copy-done.1
  101.5 0.0 copy-start
  101.5 0.7 copy.18
  102.2 0.3 copy-done
  102.5 0.7 copy.19
  (3 shorter events, 0.0 us)
Async XLA Ops:
  0.6 0.7 copy-start.3
  98.7 1.7 %copy-start.2 = (bf16[256,512]{1,0:T(8,128)(2,1)S(1)}, bf16[256,512]{1,0:T(8,128)(2,1)}, u32[]{:S(2)}) copy-start(bf16[256,512]{1,0:T(8,128)(2,1)} %get-tuple-element.12) | copy-start | bytes 786436
  100.4 1.0 %copy-start.1 = (bf16[256,512]{1,0:T(8,128)(2,1)S(1)}, bf16[256,512]{1,0:T(8,128)(2,1)}, u32[]{:S(2)}) copy-start(bf16[256,512]{1,0:T(8,128)(2,1)} %get-tuple-element.13) | copy-start | bytes 786436
  101.5 1.0 %copy-start = (f32[128,512]{1,0:T(8,128)S(1)}, f32[128,512]{1,0:T(8,128)}, u32[]{:S(2)}) copy-start(f32[128,512]{1,0:T(8,128)} %get-tuple-element.14) | copy-start | bytes 786436

commit v2 on v1

--- a/solution.py
+++ b/solution.py
@@ -11,6 +11,8 @@
 KB = 32
 LANES = 128
 CHUNK = 256
+PLANE = 4
+PARTS = 2
 NEG = -1e30
 F32 = jnp.float32
 BF16 = jnp.bfloat16
@@ -24,8 +26,8 @@
     n, nt, hs,
     q_ref, k_ref, v_ref, lse_ref, g_ref, req_ref, used_ref, x_ref,
     qg_ref, kg_ref, vg_ref, wg_ref,
-    reqbox, sel, outk, outv, kall, vall, rvo, rko, rvi, rki, wscr, ownv, ownk, bias, xall, wpart, win,
-    req_s, req_r, k_s, k_r, v_s, v_r, vt_s, vt_r, kt_s, kt_r, w_s, w_r, x_s, x_r,
+    reqbox, sel, outk, outv, kall, vall, rvo, rko, rvi, rki, wscr, ownv, ownk, bias, xall, wp, r1, r2, r3,
+    req_s, req_r, k_s, k_r, v_s, v_r, vt_s, vt_r, kt_s, kt_r, a_s, a_r, b_s, b_r, c_s, c_r, x_s, x_r,
 ):
     me = lax.axis_index("kv")
     mt = lax.axis_index("tp")
@@ -50,6 +52,7 @@
     vall[0:nf] = jnp.zeros((nf, cols), BF16)
     rvi[...] = jnp.zeros_like(rvi)
     rki[...] = jnp.zeros_like(rki)
+    wscr[:, 0:nf, :] = jnp.zeros((wscr.shape[0], nf, rows), F32)
 
     barrier = pltpu.get_barrier_semaphore()
 
@@ -80,9 +83,30 @@
     def kt_copy(src_i, dst_i):
         return rcopy(slot(rko, dst_i), slot(rki, src_i), kt_s.at[dst_i], kt_r.at[src_i], {"kv": dst_i})
 
-    def w_copy(src_i, dst_i):
-        return rcopy(wpart.at[pl.ds(pl.multiple_of(dst_i * wrows, wrows), wrows)], win.at[src_i],
-                     w_s.at[dst_i], w_r.at[src_i], {"kv": dst_i})
+    xb = lax.rem(me, 2)
+    yb = lax.rem(lax.div(me, 2), 2)
+    zi = lax.div(me, PLANE)
+    nz = n // PLANE
+    parts = wp.shape[0]
+    wrp = wrows // parts
+    px = me + 1 - 2 * xb
+    py = me + 2 - 4 * yb
+
+    def order(p):
+        return (xb, yb, px, py) if p % 2 == 0 else (yb, xb, py, px)
+
+    def a_copy(p):
+        f, _, peer, _ = order(p)
+        return rcopy(wp.at[p, pl.ds((1 - f) * 2, 2)], r1.at[p], a_s.at[p], a_r.at[p], {"kv": peer})
+
+    def b_copy(p):
+        f, g, _, peer = order(p)
+        return rcopy(wp.at[p, f * 2 + 1 - g], r2.at[p], b_s.at[p], b_r.at[p], {"kv": peer})
+
+    def c_copy(p, src_z, dst_z):
+        f, g, _, _ = order(p)
+        return rcopy(wp.at[p, f * 2 + g, dst_z], r3.at[p, src_z], c_s.at[p, dst_z], c_r.at[p, src_z],
+                     {"kv": me + (dst_z - zi) * PLANE})
 
     def x_copy(src_t, dst_t):
         return rcopy(x_ref, xall.at[src_t], x_s.at[dst_t], x_r.at[src_t], {"tp": dst_t})
@@ -106,6 +130,34 @@
     causal = (kpos <= qpos) & (kpos // QB == qpos // QB)
     bias[nf:] = jnp.where(causal, 0.0, bias[nf:])
 
+    lane_ids = lax.broadcasted_iota(jnp.int32, (1, LANES), 1)
+    masks = [
+        jnp.where((lane_ids >= s * hs) & (lane_ids < (s + 1) * hs), 1.0, 0.0).astype(BF16)
+        for s in range(hp)
+    ]
+
+    def scan_keys(start, size):
+        here = pl.ds(start, size)
+        outs = []
+        for p in range(cols // LANES):
+            at = slice(p * LANES, (p + 1) * LANES)
+            qp = q_ref[:, at] * jnp.asarray(scale, BF16)
+            gp = g_ref[:, at]
+            kp = kall[here, at]
+            terms = None
+            for s in range(hp):
+                h = p * hp + s
+                scores = dot(kp, qp * masks[s], 1, 1)
+                w = jnp.exp(scores + (bias[here, :] - lse_ref[h:h + 1, :]))
+                wscr[h, here, :] = w
+                term = dot(w.astype(BF16), gp * masks[s], 1, 0)
+                terms = term if terms is None else terms + term
+            outs.append((at, terms))
+        return outs
+
+    for at, terms in scan_keys(nf, rows):
+        ownv[:, at] = terms
+
     @pl.loop(me + 1, n)
     def _(i):
         req_copy(i, me).wait_recv()
@@ -130,35 +182,50 @@
     def _(i):
         v_copy(me, i).start()
 
-    lane_ids = lax.broadcasted_iota(jnp.int32, (1, LANES), 1)
-    masks = [
-        jnp.where((lane_ids >= s * hs) & (lane_ids < (s + 1) * hs), 1.0, 0.0).astype(BF16)
-        for s in range(hp)
-    ]
-
-    @pl.loop(0, me)
-    def _(j):
-        k_copy(j, me).wait_recv()
-
-    for p in range(cols // LANES):
-        at = slice(p * LANES, (p + 1) * LANES)
-        qp = q_ref[:, at] * jnp.asarray(scale, BF16)
-        gp = g_ref[:, at]
-        kp = kall[:, at]
-        terms = None
-        for s in range(hp):
-            h = p * hp + s
-            scores = dot(kp, qp * masks[s], 1, 1)
-            w = jnp.exp(scores + (bias[...] - lse_ref[h:h + 1, :]))
-            wscr[h] = w
-            term = dot(w.astype(BF16), gp * masks[s], 1, 0)
-            terms = term if terms is None else terms + term
-        rvo[:, at] = terms[:nf].astype(BF16)
-        ownv[:, at] = terms[nf:]
-
-    @pl.loop(0, me)
-    def _(j):
-        vt_copy(me, j).start()
+    def group(first, end):
+        @pl.loop(first, end)
+        def _(j):
+            k_copy(j, me).wait_recv()
+
+        start = pl.multiple_of(first * KB, PLANE * KB)
+        for at, terms in scan_keys(start, PLANE * KB):
+            rvo[pl.ds(start, PLANE * KB), at] = terms.astype(BF16)
+
+        @pl.loop(first, end)
+        def _(j):
+            vt_copy(me, j).start()
+
+    group(zi * PLANE, me)
+
+    @pl.loop(0, zi)
+    def _(t):
+        first = (zi - 1 - t) * PLANE
+        group(first, first + PLANE)
+
+    @pl.loop(me + 1, n)
+    def _(i):
+        vt_copy(i, me).wait_recv()
+
+    vg = (ownv[...] + dot(sel[...], rvi[...], 0, 0)).astype(BF16)
+    vg_ref[...] = vg
+
+    @pl.loop(1, nt)
+    def _(d):
+        x_copy(lax.rem(mt + d, nt), mt).wait_recv()
+
+    width = min(CHUNK, feats)
+    for t in range(nt):
+        for c in range(feats // width):
+            piece = dot(xall[t, :, c * width:(c + 1) * width], vg, 0, 0).astype(BF16)
+            for r in range(width // wrows):
+                i = (t * feats + c * width) // wrows + r
+                bx, by, bz = i % 2, (i // 2) % 2, i // PLANE
+                for p in range(parts):
+                    to = bx * 2 + by if p % 2 == 0 else by * 2 + bx
+                    wp[p, to, bz] = piece[r * wrows + p * wrp:r * wrows + (p + 1) * wrp, :]
+
+    for p in range(parts):
+        a_copy(p).start()
 
     @pl.loop(0, me)
     def _(j):
@@ -191,26 +258,22 @@
     def _(j):
         kt_copy(me, j).start()
 
-    @pl.loop(me + 1, n)
-    def _(i):
-        vt_copy(i, me).wait_recv()
-
-    vg = (ownv[...] + dot(sel[...], rvi[...], 0, 0)).astype(BF16)
-    vg_ref[...] = vg
-
-    @pl.loop(1, nt)
-    def _(d):
-        x_copy(lax.rem(mt + d, nt), mt).wait_recv()
-
-    width = min(CHUNK, feats)
-    for t in range(nt):
-        for c in range(feats // width):
-            piece = dot(xall[t, :, c * width:(c + 1) * width], vg, 0, 0)
-            wpart[t * feats + c * width:t * feats + (c + 1) * width, :] = piece.astype(BF16)
-
-    @pl.loop(1, n)
-    def _(d):
-        w_copy(me, lax.rem(me + d, n)).start()
+    for p in range(parts):
+        f, g, _, _ = order(p)
+        a_copy(p).wait()
+        half = wp[p, pl.ds(f * 2, 2)].astype(F32) + r1[p].astype(F32)
+        wp[p, pl.ds(f * 2, 2)] = half.astype(BF16)
+        b_copy(p).start()
+
+    for p in range(parts):
+        f, g, _, _ = order(p)
+        b_copy(p).wait()
+        mine = wp[p, f * 2 + g].astype(F32) + r2[p].astype(F32)
+        wp[p, f * 2 + g] = mine.astype(BF16)
+
+        @pl.loop(1, nz)
+        def _(e):
+            c_copy(p, zi, lax.rem(zi + e, nz)).start()
 
     @pl.loop(me + 1, n)
     def _(i):
@@ -218,13 +281,16 @@
 
     kg_ref[...] = (ownk[...] + dot(sel[...], rki[...], 0, 0)).astype(BF16)
 
-    wg_ref[...] = wpart[pl.ds(pl.multiple_of(me * wrows, wrows), wrows), :].astype(F32)
-
-    @pl.loop(1, n)
-    def _(d):
-        i = lax.rem(me + n - d, n)
-        w_copy(i, me).wait_recv()
-        wg_ref[...] += win[i].astype(F32)
+    for p in range(parts):
+        f, g, _, _ = order(p)
+        at = slice(p * wrp, (p + 1) * wrp)
+        wg_ref[at, :] = wp[p, f * 2 + g, zi].astype(F32)
+
+        @pl.loop(1, nz)
+        def _(e):
+            src_z = lax.rem(zi + nz - e, nz)
+            c_copy(p, src_z, zi).wait_recv()
+            wg_ref[at, :] += r3[p, src_z].astype(F32)
 
     @pl.loop(0, me)
     def _(j):
@@ -237,9 +303,10 @@
         k_copy(me, i).wait_send()
         v_copy(me, i).wait_send()
 
-    @pl.loop(1, n)
-    def _(d):
-        w_copy(me, lax.rem(me + d, n)).wait_send()
+    for p in range(parts):
+        @pl.loop(1, nz)
+        def _(e):
+            c_copy(p, zi, lax.rem(zi + e, nz)).wait_send()
 
     @pl.loop(1, nt)
     def _(d):
@@ -269,6 +336,8 @@
     slots = jnp.arange(n + key_blocks, dtype=jnp.int32)
     use = jnp.any(ids[:, :, None] == slots, axis=1).T
     used = jnp.repeat(jnp.where(use, 0.0, NEG).astype(F32), QB, axis=1)[:, None, :]
+    nz = n // PLANE
+    wrp = wrows // PARTS
     vmem = pl.BlockSpec(memory_space=pltpu.VMEM)
     dma = pltpu.SemaphoreType.DMA
     return pl.pallas_call(
@@ -297,9 +366,11 @@
             pltpu.VMEM((rows, cols), F32),
             pltpu.VMEM((nf + rows, rows), F32),
             pltpu.VMEM((nt, rows, feats), BF16),
-            pltpu.VMEM((n * wrows, cols), BF16),
-            pltpu.VMEM((n, wrows, cols), BF16),
-        ] + [dma((n,))] * 12 + [dma((nt,))] * 2,
+            pltpu.VMEM((PARTS, PLANE, nz, wrp, cols), BF16),
+            pltpu.VMEM((PARTS, 2, nz, wrp, cols), BF16),
+            pltpu.VMEM((PARTS, nz, wrp, cols), BF16),
+            pltpu.VMEM((PARTS, nz, wrp, cols), BF16),
+        ] + [dma((n,))] * 10 + [dma((PARTS,))] * 4 + [dma((PARTS, nz))] * 2 + [dma((nt,))] * 2,
         compiler_params=pltpu.CompilerParams(
             collective_id=0, has_side_effects=True, vmem_limit_bytes=60 * 1024 * 1024
         ),

time: 103 us -> 73.5 us (0.71)
  the two profiles are of different devices: /device:TPU:14 before, /device:TPU:0 now
where the time goes in v2:
time: 73.5 us; the launch traced here: 73.3 us
  Pallas kernels  65.8 us (90%)
  local copies, waits for them, and re-layouts  6.56 us (9%)
    pallas_call x1, Pallas kernels, body(): pl.pallas_call(partial(kernel, n, nt, hs), out_shape=(jax.ShapeDtypeStruc...  65.8 us
    unnamed x12, local copies, waits for them, and re-layouts  5.18 us

profile of v2, /device:TPU:0, one launch (start us, length us, event | category | flops | bytes accessed | tf_op | source)
XLA Modules:
  0.0 73.3 jit_solution(10340269368551104120)
XLA Ops:
  0.6 0.0 copy-start.3
  0.6 0.7 copy-done.3
  1.3 0.1 fusion.1
  1.4 0.1 select_reduce_fusion
  1.5 0.6 broadcast_in_dim.39.req_ref
  2.1 0.1 copy.11
  2.2 0.7 broadcast_in_dim.42
  2.9 65.8 %shard_map.102 = (bf16[256,512]{1,0:T(8,128)(2,1)}, bf16[256,512]{1,0:T(8,128)(2,1)}, bf16[256,512]{1,0:T(8,128)(2,1)}, f32[128,512]{1,0:T(8,128)}) custom-call(bf16[256,512]{1,0:T(8,128)(2,1)} %q_ref.1, bf16[256,512]{1,0:T(8,128)(2,1)} %k_ref.1, bf16[256,512]{1,0:T(8,128)(2,1)} %v_ref.1, f32[8,256]{1,0:T(8,128)} %lse_ref.1, bf16[256,512]{1,0:T(8,128)(2,1)} %g_ref.1, ...), custom_call_target="tpu_custom_call" | custom-call | tf_op jit(solution)/shard_map/pallas_call | solution.py:343
  68.8 0.0 copy-start.2
  68.8 1.7 %copy.16 = bf16[256,512]{1,0:T(8,128)(2,1)} copy(bf16[256,512]{1,0:T(8,128)(2,1)} %get-tuple-element.11) | data formatting | bytes 524288
  70.5 0.0 copy-done.2
  70.5 0.0 copy-start.1
  70.5 0.7 copy.17
  71.2 0.3 copy-done.1
  71.5 0.0 copy-start
  71.5 0.7 copy.18
  72.2 0.3 copy-done
  72.6 0.7 copy.19
  (3 shorter events, 0.0 us)
Async XLA Ops:
  0.6 0.7 copy-start.3
  68.8 1.7 %copy-start.2 = (bf16[256,512]{1,0:T(8,128)(2,1)S(1)}, bf16[256,512]{1,0:T(8,128)(2,1)}, u32[]{:S(2)}) copy-start(bf16[256,512]{1,0:T(8,128)(2,1)} %get-tuple-element.12) | copy-start | bytes 786436
  70.5 1.0 %copy-start.1 = (bf16[256,512]{1,0:T(8,128)(2,1)S(1)}, bf16[256,512]{1,0:T(8,128)(2,1)}, u32[]{:S(2)}) copy-start(bf16[256,512]{1,0:T(8,128)(2,1)} %get-tuple-element.13) | copy-start | bytes 786436
  71.5 1.0 %copy-start = (f32[128,512]{1,0:T(8,128)S(1)}, f32[128,512]{1,0:T(8,128)}, u32[]{:S(2)}) copy-start(f32[128,512]{1,0:T(8,128)} %get-tuple-element.14) | copy-start | bytes 786436

commit v3 on v2

--- a/solution.py
+++ b/solution.py
@@ -12,7 +12,6 @@
 LANES = 128
 CHUNK = 256
 PLANE = 4
-PARTS = 2
 NEG = -1e30
 F32 = jnp.float32
 BF16 = jnp.bfloat16
@@ -311,6 +310,11 @@
     @pl.loop(1, nt)
     def _(d):
         x_copy(mt, lax.rem(mt + d, nt)).wait_send()
+
+
+def settle(*refs):
+    for src, dst in zip(refs[:4], refs[4:]):
+        dst[...] = src[...]
 
 
 def body(n, nt, queries, keys, values, log_sums, out_grad, chosen, normed):
@@ -337,10 +341,11 @@
     use = jnp.any(ids[:, :, None] == slots, axis=1).T
     used = jnp.repeat(jnp.where(use, 0.0, NEG).astype(F32), QB, axis=1)[:, None, :]
     nz = n // PLANE
-    wrp = wrows // PARTS
+    parts = 4 if wrows % 64 == 0 else 2
+    wrp = wrows // parts
     vmem = pl.BlockSpec(memory_space=pltpu.VMEM)
     dma = pltpu.SemaphoreType.DMA
-    return pl.pallas_call(
+    outs = pl.pallas_call(
         partial(kernel, n, nt, hs),
         out_shape=(
             jax.ShapeDtypeStruct((rows, cols), BF16),
@@ -366,15 +371,21 @@
             pltpu.VMEM((rows, cols), F32),
             pltpu.VMEM((nf + rows, rows), F32),
             pltpu.VMEM((nt, rows, feats), BF16),
-            pltpu.VMEM((PARTS, PLANE, nz, wrp, cols), BF16),
-            pltpu.VMEM((PARTS, 2, nz, wrp, cols), BF16),
-            pltpu.VMEM((PARTS, nz, wrp, cols), BF16),
-            pltpu.VMEM((PARTS, nz, wrp, cols), BF16),
-        ] + [dma((n,))] * 10 + [dma((PARTS,))] * 4 + [dma((PARTS, nz))] * 2 + [dma((nt,))] * 2,
+            pltpu.VMEM((parts, PLANE, nz, wrp, cols), BF16),
+            pltpu.VMEM((parts, 2, nz, wrp, cols), BF16),
+            pltpu.VMEM((parts, nz, wrp, cols), BF16),
+            pltpu.VMEM((parts, nz, wrp, cols), BF16),
+        ] + [dma((n,))] * 10 + [dma((parts,))] * 4 + [dma((parts, nz))] * 2 + [dma((nt,))] * 2,
         compiler_params=pltpu.CompilerParams(
             collective_id=0, has_side_effects=True, vmem_limit_bytes=60 * 1024 * 1024
         ),
     )(queries, keys, values, log_sums, out_grad, req, used, normed)
+    return pl.pallas_call(
+        settle,
+        out_shape=tuple(jax.ShapeDtypeStruct(o.shape, o.dtype) for o in outs),
+        in_specs=[vmem] * 4,
+        out_specs=(vmem,) * 4,
+    )(*outs)
 
 
 def solution(mesh):

time: 73.5 us -> 67.7 us (0.921)
  local copies, waits for them, and re-layouts: 6.56 us -> 2.05 us
  Pallas kernels: 65.8 us -> 63.9 us
    unnamed x12 -> x2, local copies, waits for them, and re-layouts: 5.18 us -> 0.67 us
    pallas_call x1, Pallas kernels: 65.8 us -> 61.8 us  [body(): pl.pallas_call(partial(kernel, n, nt, hs), out_shape=(jax.ShapeDtypeStruc...]
    pallas_call x0 -> x1, Pallas kernels: none -> 2.17 us  [body(): pl.pallas_call(settle, out_shape=tuple((jax.ShapeDtypeStruct(o.shape, o.d...]
where the time goes in v3:
time: 67.7 us; the launch traced here: 66.9 us
  Pallas kernels  63.9 us (94%)
  local copies, waits for them, and re-layouts  2.05 us (3%)
    pallas_call x1, Pallas kernels, body(): pl.pallas_call(partial(kernel, n, nt, hs), out_shape=(jax.ShapeDtypeStruc...  61.8 us
    pallas_call x1, Pallas kernels, body(): pl.pallas_call(settle, out_shape=tuple((jax.ShapeDtypeStruct(o.shape, o.d...  2.17 us

profile of v3, /device:TPU:0, one launch (start us, length us, event | category | flops | bytes accessed | tf_op | source)
XLA Modules:
  0.0 66.9 jit_solution(17003843193500586375)
XLA Ops:
  0.6 0.0 copy-start
  0.6 0.7 %copy-done = s32[2,8]{1,0:T(2,128)S(1)} copy-done((s32[2,8]{1,0:T(2,128)S(1)}, s32[2,8]{1,0:T(2,128)}, u32[]{:S(2)}) %copy-start) | copy-done | bytes 88
  1.3 0.1 fusion.1
  1.4 0.1 select_reduce_fusion
  1.5 0.6 broadcast_in_dim.39.req_ref
  2.1 0.1 copy.11
  2.2 0.7 %broadcast_in_dim.42 = f32[24,2,128]{2,1,0:T(2,128)} broadcast(f32[24,2]{1,0:T(8,128)S(1)} %copy.11), dimensions={0,1} | broadcast | bytes 24768 | tf_op jit(solution)/shard_map/broadcast_in_dim | solution.py:342
  2.9 61.8 %shard_map.102 = (bf16[256,512]{1,0:T(8,128)(2,1)}, bf16[256,512]{1,0:T(8,128)(2,1)}, bf16[256,512]{1,0:T(8,128)(2,1)}, f32[128,512]{1,0:T(8,128)}) custom-call(bf16[256,512]{1,0:T(8,128)(2,1)} %q_ref.1, bf16[256,512]{1,0:T(8,128)(2,1)} %k_ref.1, bf16[256,512]{1,0:T(8,128)(2,1)} %v_ref.1, f32[8,256]{1,0:T(8,128)} %lse_ref.1, bf16[256,512]{1,0:T(8,128)(2,1)} %g_ref.1, ...), custom_call_target="tpu_custom_call" | custom-call | tf_op jit(solution)/shard_map/pallas_call | solution.py:348
  64.7 2.2 %shard_map.103 = (bf16[256,512]{1,0:T(8,128)(2,1)}, bf16[256,512]{1,0:T(8,128)(2,1)}, bf16[256,512]{1,0:T(8,128)(2,1)}, f32[128,512]{1,0:T(8,128)}) custom-call(bf16[256,512]{1,0:T(8,128)(2,1)} %get-tuple-element.8.refs_0_, bf16[256,512]{1,0:T(8,128)(2,1)} %get-tuple-element.9.refs_1_, bf16[256,512]{1,0:T(8,128)(2,1)} %get-tuple-element.10.refs_2_, ...), custom_call_target="tpu_custom_call" | custom-call | tf_op jit(solution)/shard_map/pallas_call | solution.py:383
  (3 shorter events, 0.0 us)
Async XLA Ops:
  0.6 0.7 %copy-start = (s32[2,8]{1,0:T(2,128)S(1)}, s32[2,8]{1,0:T(2,128)}, u32[]{:S(2)}) copy-start(s32[2,8]{1,0:T(2,128)} %param.12) | copy-start | bytes 196
